TPU v7x, 512 devices: a whole 4x4x16 slice. The times are simulated.
512 devices in a mesh: ep: 32 (over z, core), tp: 16 (over y, x).
Axes of the slice: x: 4, y: 4, z: 16, core: 2. Of those that a mesh axis runs over, the one named last changes fastest.
Arguments:
- tokens: bfloat16 [65536, 2048], P(('ep', 'tp')), may hold values from -6 to 6
- norm_gain: float32 [2048], replicated, may hold values from 0.1 to 1.9
- expert_ids: int32 [65536, 2], P(('ep', 'tp')), may hold values from 0 to 31, all different within a row; in each aligned block of 128 rows (0 to 127, 128 to 255, ...) at most 16 rows name the same one
- gate_weights: float32 [65536, 2], P(('ep', 'tp')), may hold values from 0.2 to 1.6
- expert_gate: bfloat16 [32, 512, 2048], P('ep', 'tp'), may hold values from -0.125 to 0.125
- expert_up: bfloat16 [32, 512, 2048], P('ep', 'tp'), may hold values from -0.125 to 0.125
- expert_down: bfloat16 [32, 512, 2048], P('ep', 'tp'), may hold values from -0.25 to 0.25
- shared_gate: bfloat16 [512, 2048], P('tp'), may hold values from -0.125 to 0.125
- shared_up: bfloat16 [512, 2048], P('tp'), may hold values from -0.125 to 0.125
- shared_down: bfloat16 [512, 2048], P('tp'), may hold values from -0.25 to 0.25
Outputs:
- mixed: bfloat16 [65536, 2048], P(('ep', 'tp'))
Inputs may be any that keep to these rules, and one draw needn't show every extreme that they name: `expert_ids`: each row names 2 different experts. Within the rows of one device no expert is named by more than 16 rows, and in every draw some expert is named by exactly 16 rows of some device.
All inputs are finite; a program needn't handle non-finite values.
Results may differ from a plain program's by a relative error of at most 0.0068.
Values may be sent and summed in bfloat16 or wider, within the bound.
A program may use at most 64 MiB of HBM per device.

v0:
```python
import jax
import jax.numpy as jnp
from jax import lax
from jax.sharding import PartitionSpec as P

EPS = 1e-06


def sent_together(arrays, axis, dim, along):
    widths = [a.shape[along] for a in arrays]
    both = jnp.concatenate(arrays, axis=along)
    result = lax.all_gather(both, axis, axis=dim, tiled=True)
    return tuple(jnp.split(result, [sum(widths[:k]) for k in range(1, len(widths))], axis=along))


def against(rows, weight):
    return lax.dot_general(
        rows, weight, (((1,), (1,)), ((), ())), preferred_element_type=jnp.float32
    )


def hidden_block(rows, gate_rows, up_rows):
    return (jax.nn.silu(against(rows, gate_rows)) * against(rows, up_rows)).astype(jnp.bfloat16)


def whole_mlp(rows, pieces):
    hidden = hidden_block(rows, pieces[0], pieces[1])
    return jnp.dot(hidden, pieces[2], preferred_element_type=jnp.float32)


def body(
    tokens,
    norm_gain,
    expert_ids,
    gate_weights,
    expert_gate,
    expert_up,
    expert_down,
    shared_gate,
    shared_up,
    shared_down,
):
    tok = tokens.astype(jnp.float32)
    normed = (
        tok * lax.rsqrt(jnp.mean(tok * tok, axis=-1, keepdims=True) + EPS) * norm_gain
    ).astype(jnp.bfloat16)
    count = lax.axis_size("ep")
    tok_rows, chosen = expert_ids.shape
    features = tokens.shape[1]
    capacity = 2 * tok_rows * chosen // count
    labels = jnp.arange(count, dtype=jnp.int32)
    hits = jnp.sum((expert_ids[:, :, None] == labels[None, None, :]).astype(jnp.int32), axis=1)
    before = jnp.cumsum(hits, axis=0) - hits
    slot_of = jnp.take_along_axis(before, expert_ids, axis=1)
    flat_pos = expert_ids * capacity + slot_of
    slots = jnp.arange(count * capacity, dtype=jnp.int32)
    placing = jnp.any(flat_pos[:, :, None] == slots[None, None, :], axis=1).astype(jnp.bfloat16)
    outgoing = lax.dot_general(
        placing, normed, (((0,), (0,)), ((), ())), preferred_element_type=jnp.float32
    )
    outgoing = outgoing.astype(jnp.bfloat16).reshape(count, capacity, features)
    arrived = lax.all_to_all(outgoing, "ep", split_axis=0, concat_axis=0, tiled=True)
    rows = arrived.reshape(count * capacity, features)
    results = whole_mlp(
        rows, sent_together((expert_gate[0], expert_up[0], expert_down[0]), "tp", 0, 1)
    )
    results = results.astype(jnp.bfloat16).reshape(count, capacity, features)
    returned = lax.all_to_all(results, "ep", split_axis=0, concat_axis=0, tiled=True).reshape(
        count * capacity, features
    )
    picked = jnp.take(returned, flat_pos.reshape(-1), axis=0).reshape(tok_rows, chosen, features)
    routed = jnp.sum(gate_weights[:, :, None] * picked.astype(jnp.float32), axis=1)
    shared = whole_mlp(normed, sent_together((shared_gate, shared_up, shared_down), "tp", 0, 1))
    return (routed + shared).astype(jnp.bfloat16)


def solution(mesh):
    in_specs = (
        P(("ep", "tp"), None),
        P(),
        P(("ep", "tp"), None),
        P(("ep", "tp"), None),
        P("ep", "tp", None),
        P("ep", "tp", None),
        P("ep", "tp", None),
        P("tp", None),
        P("tp", None),
        P("tp", None),
    )
    out_specs = P(("ep", "tp"), None)
    return jax.shard_map(body, mesh=mesh, in_specs=in_specs, out_specs=out_specs, check_vma=False)
```

profile of v0, /device:TPU:44, one launch (start us, length us, event | category | flops | bytes accessed | tf_op | source)
XLA Modules:
  0.0 262.0 jit_solution(10791896016266745345)
XLA Ops:
  6.5 1.8 pad_maximum_fusion
  8.4 0.7 convert_reduce_fusion
  9.1 0.1 copy.36
  9.2 0.2 reduce_window_sum.11
  9.3 0.7 bitcast_or_fusion
  10.0 0.1 copy.38
  10.1 0.1 reshape.90
  10.3 1.9 gather_fusion.1
  12.3 0.1 reshape.93
  12.4 0.1 copy.39
  12.5 0.1 fusion.34
  12.6 0.2 fusion.25
  12.9 2.2 convolution_convert_fusion.1
  15.0 15.5 %all-to-all-start = ((bf16[32,16,2048]{2,1,0:T(8,128)(2,1)}), bf16[32,16,2048]{2,1,0:T(8,128)(2,1)S(1)}, u32[]{:S(2)}, u32[]{:S(2)}) async-start(bf16[32,16,2048]{2,1,0:T(8,128)(2,1)} %bitcast.1), calls=%async_computation | async-start | bytes 4194304 | tf_op jit(solution)/shard_map/all_to_all | solution.py:62
  30.5 0.0 all-gather.5.cloned.1.call-start
  30.6 0.8 pad_maximum_fusion.1
  31.4 0.0 all-gather.5.cloned.1.call-update
  31.4 99.2 %all-to-all-done = bf16[32,16,2048]{2,1,0:T(8,128)(2,1)S(1)} async-done(((bf16[32,16,2048]{2,1,0:T(8,128)(2,1)}), bf16[32,16,2048]{2,1,0:T(8,128)(2,1)S(1)}, u32[]{:S(2)}, u32[]{:S(2)}) %all-to-all-start) | async-done | bytes 2097184 | tf_op jit(solution)/shard_map/all_to_all | solution.py:62
  130.6 3.9 %fusion.9 = f32[512,512]{1,0:T(8,128)} fusion(bf16[512,2048]{1,0:T(8,128)(2,1)S(1)} %bitcast.16, bf16[512,6144]{1,0:T(8,128)(2,1)} %all-gather.3.cloned.1.call-done), kind=kOutput, calls=%fused_computation.14 | convolution fusion | flops 1073741824 | bytes 5242880 | tf_op jit(solution)/shard_map/dot_general | solution.py:17
  134.4 6.4 %convolution_convert_fusion = bf16[512,2048]{1,0:T(8,128)(2,1)} fusion(bf16[512,6144]{1,0:T(8,128)(2,1)} %all-gather.3.cloned.1.call-done, bf16[512,2048]{1,0:T(8,128)(2,1)S(1)} %bitcast.17, f32[512,512]{1,0:T(8,128)} %fusion.9), kind=kOutput, calls=%fused_computation.2 | convolution fusion | flops 2150105088 | bytes 9437184 | tf_op jit(solution)/shard_map/dot_general | solution.py:28
  140.8 3.9 %all-to-all-start.1 = ((bf16[32,16,2048]{2,1,0:T(8,128)(2,1)}), bf16[32,16,2048]{2,1,0:T(8,128)(2,1)S(1)}, u32[]{:S(2)}, u32[]{:S(2)}) async-start(bf16[32,16,2048]{2,1,0:T(8,128)(2,1)} %bitcast.18), calls=%async_computation.1 | async-start | bytes 4194304 | tf_op jit(solution)/shard_map/all_to_all | solution.py:68
  144.8 0.1 copy.41
  144.9 0.1 reshape.81
  145.0 0.1 copy.40
  145.2 0.1 copy.35
  145.3 23.5 %all-gather.5.cloned.1.call-done = bf16[512,6144]{1,0:T(8,128)(2,1)} async-done(((bf16[32,6144]{1,0:T(8,128)(2,1)}), bf16[512,6144]{1,0:T(8,128)(2,1)}) %all-gather.5.cloned.1.call-update) | async-done | bytes 6291472 | tf_op jit(solution)/shard_map/all_gather | solution.py:12
  168.8 2.4 fusion.4
  171.3 73.4 %all-to-all-done.1 = bf16[32,16,2048]{2,1,0:T(8,128)(2,1)S(1)} async-done(((bf16[32,16,2048]{2,1,0:T(8,128)(2,1)}), bf16[32,16,2048]{2,1,0:T(8,128)(2,1)S(1)}, u32[]{:S(2)}, u32[]{:S(2)}) %all-to-all-start.1) | async-done | bytes 2097184 | tf_op jit(solution)/shard_map/all_to_all | solution.py:68
  244.7 1.4 gather_fusion
  246.1 0.7 gather.12
  246.8 4.1 %multiply_reduce_fusion = f32[128,2048]{1,0:T(8,128)S(1)} fusion(bf16[128,2,2048]{2,1,0:T(2,128)(2,1)S(1)} %gather.12, pred[128,2]{1,0:T(8,128)(4,1)S(1)} %copy.40, f32[128,2]{1,0:T(8,128)S(1)} %copy.35), kind=kLoop, calls=%fused_computation.16 | loop fusion | flops 1835008 | bytes 2098432 | tf_op jit(solution)/shard_map/reduce_sum | solution.py:72
  250.9 4.3 %fusion = bf16[128,2048]{1,0:T(8,128)(2,1)} fusion(f32[128,2048]{1,0:T(8,128)S(1)} %multiply_reduce_fusion, bf16[512,6144]{1,0:T(8,128)(2,1)} %all-gather.5.cloned.1.call-done, f32[128,512]{1,0:T(8,128)S(1)} %fusion.4, bf16[128,2048]{1,0:T(8,128)(2,1)S(1)} %copy-done.1, f32[2048]{0:T(1024)S(1)} %copy-done.6, f32[128]{0:T(128)S(1)} %add_rsqrt_fusion), kind=kOutput, calls=%fused_computation.5 | convolution fusion | flops 538836992 | bytes 6562304 | tf_op jit(solution)/shard_map/dot_general | solution.py:28
  (24 shorter events, 0.1 us)
Async XLA Ops:
  6.5 124.0 %all-gather.3.cloned.1.call-start = ((), (), s32[]{:S(2)}) async-start(), calls=%async_computation.2 | async-start | bytes 6684672 | tf_op jit(solution)/shard_map/all_gather | solution.py:12
  10.3 2.2 copy-start.5
  10.3 2.3 copy-start
  10.3 2.5 copy-start.6
  15.0 15.6 %copy-start.2 = (bf16[32,2048]{1,0:T(8,128)(2,1)S(1)}, bf16[32,2048]{1,0:T(8,128)(2,1)}, u32[]{:S(2)}) copy-start(bf16[32,2048]{1,0:T(8,128)(2,1)} %param.19) | copy-start | bytes 393220
  15.0 15.6 %copy-start.3 = (bf16[32,2048]{1,0:T(8,128)(2,1)S(1)}, bf16[32,2048]{1,0:T(8,128)(2,1)}, u32[]{:S(2)}) copy-start(bf16[32,2048]{1,0:T(8,128)(2,1)} %param.18) | copy-start | bytes 393220
  15.0 15.6 %copy-start.4 = (bf16[32,2048]{1,0:T(8,128)(2,1)S(1)}, bf16[32,2048]{1,0:T(8,128)(2,1)}, u32[]{:S(2)}) copy-start(bf16[32,2048]{1,0:T(8,128)(2,1)} %param.17) | copy-start | bytes 393220
  15.0 115.6 %all-to-all-start = ((bf16[32,16,2048]{2,1,0:T(8,128)(2,1)}), bf16[32,16,2048]{2,1,0:T(8,128)(2,1)S(1)}, u32[]{:S(2)}, u32[]{:S(2)}) async-start(bf16[32,16,2048]{2,1,0:T(8,128)(2,1)} %bitcast.1), calls=%async_computation | async-start | bytes 4194304 | tf_op jit(solution)/shard_map/all_to_all | solution.py:62
  30.5 138.3 %all-gather.5.cloned.1.call-start = ((), (), s32[]{:S(2)}) async-start(), calls=%async_computation.3 | async-start | bytes 6684672 | tf_op jit(solution)/shard_map/all_gather | solution.py:12
  140.8 4.3 %copy-start.7 = (f32[128,2]{0,1:T(2,128)S(1)}, f32[128,2]{0,1:T(2,128)}, u32[]{:S(2)}) copy-start(f32[128,2]{0,1:T(2,128)} %param.13) | copy-start | bytes 3076
  140.8 103.9 %all-to-all-start.1 = ((bf16[32,16,2048]{2,1,0:T(8,128)(2,1)}), bf16[32,16,2048]{2,1,0:T(8,128)(2,1)S(1)}, u32[]{:S(2)}, u32[]{:S(2)}) async-start(bf16[32,16,2048]{2,1,0:T(8,128)(2,1)} %bitcast.18), calls=%async_computation.1 | async-start | bytes 4194304 | tf_op jit(solution)/shard_map/all_to_all | solution.py:68
  246.1 4.8 %copy-start.1 = (bf16[128,2048]{1,0:T(8,128)(2,1)S(1)}, bf16[128,2048]{1,0:T(8,128)(2,1)}, u32[]{:S(2)}) copy-start(bf16[128,2048]{1,0:T(8,128)(2,1)} %param.10) | copy-start | bytes 1572868
Sparse Core Ops, SparseCore 0:
  10.3 79.0 all-gather.2
  92.4 76.3 all-gather.4
where the time goes:
time: 262 us
  waiting for transfers between devices  196 us (75%)
  starting transfers between devices  19.5 us (7%)
  matrix products  19.1 us (7%)
  between operations  13.6 us (5%)
  other arithmetic  8.55 us (3%)
  local copies, waits for them, and re-layouts  5.11 us (2%)
    all_to_all x1, waiting for transfers between devices, body(): lax.all_to_all(outgoing, 'ep', split_axis=0, concat_axis=0, tiled=True)  99.2 us
    all_to_all x1, waiting for transfers between devices, body(): lax.all_to_all(results, 'ep', split_axis=0, concat_axis=0, tiled=True)  73.4 us
    all_gather x2, waiting for transfers between devices, sent_together(): result = lax.all_gather(both, axis, axis=dim, tiled=True)  23.5 us
    all_to_all x1, starting transfers between devices, body(): lax.all_to_all(outgoing, 'ep', split_axis=0, concat_axis=0, tiled=True)  15.5 us
    dot_general x2, matrix products, whole_mlp(): return jnp.dot(hidden, pieces[2], preferred_element_type=jnp.float32)  10.6 us
    dot_general x2, matrix products, against(): lax.dot_general(rows, weight, (((1,), (1,)), ((), ())), preferred_element...  6.28 us
  transfers between devices with their start and end apart: 4, of which 3 were waited for; matrix products, arithmetic and copies ran while one was open for 8% of the time, Pallas kernels for 0%

commit v1 on v0

v1 whole, which is shorter than its diff:
```python
import functools

import jax
import jax.numpy as jnp
from jax import lax
from jax.experimental import pallas as pl
from jax.experimental.pallas import tpu as pltpu
from jax.sharding import PartitionSpec as P

EPS = 1e-06
MESH = pl.DeviceIdType.MESH
BF = jnp.bfloat16
F32 = jnp.float32
NX = 4
NZ = 16
TOK = 128
D = 2048
CAP = 16
NE = 32
COLS = 512
ND = D // COLS
NT = (((1,), (1,)), ((), ()))


def kernel(
    tokens, gain, ids, gw, eg, eu, ed, shg, shu, shd, out,
    tok, xt, meta, sw, part, pin, own, placed, rows, hid, wgu, wd, res, ret, wt, outb,
    zrecv, zsend, gsend, loc, xrecv, mrecv, srecv, prow, pinr, retr, sends, osem,
):
    ep, p = lax.axis_index("ep"), lax.axis_index("tp")
    z, c = ep // 2, ep % 2
    x, y = p % NX, p // NX
    delta = (z - (p + 8 * c) + 2 * NZ) % NZ
    go_up = delta <= 7
    go_down = (delta == 0) | (delta >= 10)
    ep_up = ((z + 1) % NZ) * 2 + c
    ep_down = ((z + NZ - 1) % NZ) * 2 + c
    target = (z + 8 * c) % NZ
    here = p == target

    def arrived(ref, sem):
        pltpu.make_async_copy(ref, ref, sem).wait()

    def send(src, dst, ssem, rsem, device):
        pltpu.make_async_remote_copy(
            src_ref=src, dst_ref=dst, send_sem=ssem, recv_sem=rsem,
            device_id=device, device_id_type=MESH,
        ).start()

    pltpu.make_async_copy(tokens, tok, loc).start()
    for m, ref in enumerate((shg, shu, shd)):
        pltpu.make_async_copy(ref, sw.at[m, y], srecv.at[y]).start()

    barrier = pltpu.get_barrier_semaphore()

    def greet(i, carry):
        @pl.when(jnp.logical_or(i // 2 != p, i % 2 != c))
        def _():
            pl.semaphore_signal(barrier, inc=1, device_id=(z * 2 + i % 2, i // 2), device_id_type=MESH)
        return carry

    lax.fori_loop(0, NE, greet, 0)
    pl.semaphore_signal(barrier, inc=1, device_id=(ep_up, p), device_id_type=MESH)
    pl.semaphore_signal(barrier, inc=1, device_id=(ep_down, p), device_id_type=MESH)
    pl.semaphore_wait(barrier, NE + 1)

    pieces = []
    for r in range(2):
        pieces.append((eg.at[r], wgu.at[0, r, p], r * 32 + p * 2))
        pieces.append((eu.at[r], wgu.at[1, r, p], r * 32 + p * 2 + 1))
    for n in range(ND):
        cols = pl.ds(n * COLS, COLS)
        pieces.append((ed.at[:, :, cols], wd.at[:, p, :, cols], 64 + n * 16 + p))

    @pl.when(here)
    def _():
        for src, dst, k in pieces:
            pltpu.make_async_copy(src, dst, zrecv.at[k]).start()

    @pl.when(jnp.logical_not(here))
    def _():
        for src, dst, k in pieces:
            send(src, dst, gsend, zrecv.at[k], (ep, target))

    ids0, ids1 = ids[0:1, :], ids[1:2, :]
    e_iota = lax.broadcasted_iota(jnp.int32, (NE, TOK), 0)
    h0 = e_iota == ids0
    h1 = e_iota == ids1
    one, zero = jnp.float32(1), jnp.float32(0)
    hits = (jnp.where(h0, one, zero) + jnp.where(h1, one, zero)).astype(BF)
    earlier = jnp.where(
        lax.broadcasted_iota(jnp.int32, (TOK, TOK), 0) < lax.broadcasted_iota(jnp.int32, (TOK, TOK), 1), one, zero
    ).astype(BF)
    before = jnp.dot(hits, earlier, preferred_element_type=F32)
    slot0 = jnp.sum(jnp.where(h0, before, zero), axis=0, keepdims=True)
    slot1 = jnp.sum(jnp.where(h1, before, zero), axis=0, keepdims=True)
    pos0 = ids0.astype(F32) * CAP + slot0
    pos1 = ids1.astype(F32) * CAP + slot1
    sub = lax.broadcasted_iota(jnp.int32, (8, TOK), 0)
    meta[x] = jnp.where(sub == 0, jnp.broadcast_to(pos0, (8, TOK)), jnp.broadcast_to(pos1, (8, TOK)))

    pltpu.make_async_copy(tokens, tok, loc).wait()
    g = gain[...]

    def norm(i, carry):
        at = pl.ds(pl.multiple_of(i * 16, 16), 16)
        t = tok[at, :].astype(F32)
        scale = lax.rsqrt(jnp.mean(t * t, axis=-1, keepdims=True) + EPS)
        xt[x, at, :] = (t * scale * g).astype(BF)
        return carry

    lax.fori_loop(0, TOK // 16, norm, 0)
    for i in (1, 3, 2):
        peer = (ep, y * NX + (x + i) % NX)
        send(meta.at[x], meta.at[x], sends.at[0], mrecv.at[x], peer)
        send(xt.at[x], xt.at[x], sends.at[1], xrecv.at[x], peer)
    for i in (1, 3, 2):
        peer = (ep, ((y + i) % NX) * NX + x)
        for m, ref in enumerate((shg, shu, shd)):
            send(ref, sw.at[m, y], sends.at[2], srecv.at[y], peer)

    slot_iota = lax.broadcasted_iota(jnp.int32, (NE * CAP, TOK), 0).astype(F32)
    w = jnp.where(slot_iota == pos0, gw[0:1, :], zero) + jnp.where(slot_iota == pos1, gw[1:2, :], zero)
    w = w.T
    w_hi = w.astype(BF)
    wt[0] = w_hi
    wt[1] = (w - w_hi.astype(F32)).astype(BF)

    def place(i):
        s = (x + i) % NX
        if i:
            arrived(meta.at[s], mrecv.at[s])
            arrived(xt.at[s], xrecv.at[s])
        row = lax.broadcasted_iota(jnp.int32, (TOK, TOK), 0)
        dest, slot = row >> 4, row & 15
        dy, dc = dest >> 1, dest & 1
        expert = 2 * ((4 * dy + x + 8 * dc) & 15) + dc
        aim = (expert * CAP + slot).astype(F32)
        m = meta[s]
        onehot = jnp.where((aim == m[0:1, :]) | (aim == m[1:2, :]), one, zero).astype(BF)
        for j in range(ND):
            cols = pl.ds(j * COLS, COLS)
            placed[s, :, :, cols] = (
                jnp.dot(onehot, xt[s, :, cols], preferred_element_type=F32).astype(BF).reshape(8, CAP, COLS)
            )
        src = (y * 2 + c) * NX + s
        rows[src] = placed[s, y * 2 + c]
        for q in range(1, 8):
            dest = (y * 2 + c + q) % 8
            send(placed.at[s, dest], rows.at[src], sends.at[3], prow, (z * 2 + dest % 2, (dest // 2) * NX + x))

    def shared(i):
        s = (x + i) % NX
        if i == 0:
            for q in range(NX):
                arrived(sw.at[:, q], srecv.at[q])
        blk = xt[s]
        a = lax.dot_general(blk, sw[0].reshape(TOK, D), NT, preferred_element_type=F32)
        b = lax.dot_general(blk, sw[1].reshape(TOK, D), NT, preferred_element_type=F32)
        h = (a / (1.0 + jnp.exp(-a)) * b).astype(BF)
        down = sw.at[2]
        for j in range(ND):
            cols = pl.ds(j * COLS, COLS)
            v = jnp.dot(h, down[:, :, cols].reshape(TOK, COLS), preferred_element_type=F32)
            if i == 0:
                own[:, cols] = v
            else:
                part[s, :, cols] = v.astype(BF)
        if i:
            send(part.at[s], pin.at[x], sends.at[4], pinr.at[x], (ep, y * NX + s))

    def hidden(r, b):
        if r == 0 and b == 0:
            arrived(rows.at[pl.ds(0, 28)], prow)
        blk = rows[8 * b:8 * b + 8].reshape(TOK, D)
        a = lax.dot_general(blk, wgu[0, r].reshape(256, D), NT, preferred_element_type=F32)
        u = lax.dot_general(blk, wgu[1, r].reshape(256, D), NT, preferred_element_type=F32)
        hid[r, b * TOK:(b + 1) * TOK, :] = (a / (1.0 + jnp.exp(-a)) * u).astype(BF)

    def pass_on(ref, k, which):
        arrived(ref, zrecv.at[k])

        @pl.when(go_up)
        def _():
            send(ref, ref, zsend.at[which], zrecv.at[k], (ep_up, p))

        @pl.when(go_down)
        def _():
            send(ref, ref, zsend.at[2 + which], zrecv.at[k], (ep_down, p))

    def gu_step(k, carry):
        pass_on(wgu.at[k % 2, k // 32, (k % 32) // 2], k, 0)
        return carry

    def run_gu(a, b):
        lax.fori_loop(a, b, gu_step, 0)

    place(0)
    run_gu(0, 4)
    place(1)
    run_gu(4, 7)
    place(3)
    run_gu(7, 12)
    place(2)
    run_gu(12, 18)
    shared(0)
    run_gu(18, 22)
    shared(1)
    run_gu(22, 26)
    shared(3)
    run_gu(26, 32)
    shared(2)
    run_gu(32, 52)
    hidden(0, 0)
    run_gu(52, 56)
    hidden(0, 1)
    run_gu(56, 60)
    hidden(0, 2)
    run_gu(60, 64)
    hidden(0, 3)

    me = 2 * ((p + 8 * c) % NZ) + c
    me_src = (y * 2 + c) * NX + x
    for n in range(ND):
        cols = pl.ds(n * COLS, COLS)

        def d_step(s, carry):
            pass_on(wd.at[:, s, :, cols], 64 + n * 16 + s, 1)
            return carry

        if n == 0:
            for b in range(4):
                lax.fori_loop(4 * b, 4 * b + 4, d_step, 0)
                hidden(1, b)
        else:
            lax.fori_loop(0, 16, d_step, 0)
        for b in range(4):
            at = pl.ds(b * TOK, TOK)
            v = jnp.dot(hid[0, at, :], wd[0, :, :, cols].reshape(256, COLS), preferred_element_type=F32)
            v = v + jnp.dot(hid[1, at, :], wd[1, :, :, cols].reshape(256, COLS), preferred_element_type=F32)
            res[8 * b:8 * b + 8, :, cols] = v.astype(BF).reshape(8, CAP, COLS)

        ret[me, :, cols] = res[me_src, :, cols]

        def give_back(i, carry):
            q = (me_src + i) % NE
            qy, qc, qx = q // 8, (q // 4) % 2, q % 4
            send(res.at[q, :, cols], ret.at[me, :, cols], sends.at[5], retr.at[n], (z * 2 + qc, qy * NX + qx))
            return carry

        lax.fori_loop(1, NE, give_back, 0)

    for i in (1, 3, 2):
        s = (x + i) % NX
        arrived(pin.at[s], pinr.at[s])
        for j in range(ND):
            cols = pl.ds(j * COLS, COLS)
            own[:, cols] = own[:, cols] + pin[s, :, cols].astype(F32)

    for n in range(ND):
        cols = pl.ds(n * COLS, COLS)
        arrived(ret.at[pl.ds(0, NE - 1), :, cols], retr.at[n])
        blk = ret[:, :, cols].reshape(NE * CAP, COLS)
        v = jnp.dot(wt[0], blk, preferred_element_type=F32) + jnp.dot(wt[1], blk, preferred_element_type=F32)
        outb[:, cols] = (v + own[:, cols]).astype(BF)
        pltpu.make_async_copy(outb.at[:, cols], out.at[:, cols], osem.at[n]).start()

    @pl.when(jnp.logical_not(here))
    def _():
        arrived(wgu.at[0, 0, pl.ds(0, 6)], gsend)

    @pl.when(go_up)
    def _():
        arrived(wgu, zsend.at[0])
        arrived(wd, zsend.at[1])

    @pl.when(go_down)
    def _():
        arrived(wgu, zsend.at[2])
        arrived(wd, zsend.at[3])

    arrived(meta.at[pl.ds(0, 3)], sends.at[0])
    arrived(xt.at[pl.ds(0, 3)], sends.at[1])
    arrived(sw.at[:, pl.ds(0, 3)], sends.at[2])
    arrived(rows.at[pl.ds(0, 28)], sends.at[3])
    arrived(pin.at[pl.ds(0, 3)], sends.at[4])
    arrived(ret.at[pl.ds(0, NE - 1)], sends.at[5])
    for n in range(ND):
        cols = pl.ds(n * COLS, COLS)
        pltpu.make_async_copy(outb.at[:, cols], out.at[:, cols], osem.at[n]).wait()


def body(tokens, norm_gain, expert_ids, gate_weights, expert_gate, expert_up, expert_down, shared_gate, shared_up, shared_down):
    anywhere = pl.BlockSpec(memory_space=pl.ANY)
    vmem = pl.BlockSpec(memory_space=pltpu.VMEM)
    dma = pltpu.SemaphoreType.DMA
    return pl.pallas_call(
        kernel,
        out_shape=jax.ShapeDtypeStruct((TOK, D), BF),
        in_specs=[anywhere, vmem, vmem, vmem] + [anywhere] * 6,
        out_specs=anywhere,
        scratch_shapes=[
            pltpu.VMEM((TOK, D), BF),
            pltpu.VMEM((NX, TOK, D), BF),
            pltpu.VMEM((NX, 8, TOK), F32),
            pltpu.VMEM((3, NX, 32, D), BF),
            pltpu.VMEM((NX, TOK, D), BF),
            pltpu.VMEM((NX, TOK, D), BF),
            pltpu.VMEM((TOK, D), F32),
            pltpu.VMEM((NX, 8, CAP, D), BF),
            pltpu.VMEM((NE, CAP, D), BF),
            pltpu.VMEM((2, NE * CAP, 256), BF),
            pltpu.VMEM((2, 2, 16, 16, D), BF),
            pltpu.VMEM((2, 16, 16, D), BF),
            pltpu.VMEM((NE, CAP, D), BF),
            pltpu.VMEM((NE, CAP, D), BF),
            pltpu.VMEM((2, TOK, NE * CAP), BF),
            pltpu.VMEM((TOK, D), BF),
            dma((128,)),
            dma((4,)),
            dma,
            dma,
            dma((NX,)),
            dma((NX,)),
            dma((NX,)),
            dma,
            dma((NX,)),
            dma((ND,)),
            dma((6,)),
            dma((ND,)),
        ],
        compiler_params=pltpu.CompilerParams(
            collective_id=0, has_side_effects=True, vmem_limit_bytes=48 * 1024 * 1024
        ),
    )(
        tokens,
        norm_gain.reshape(1, D),
        expert_ids.T,
        gate_weights.T,
        expert_gate.reshape(2, 16, D),
        expert_up.reshape(2, 16, D),
        expert_down.reshape(2, 16, D),
        shared_gate,
        shared_up,
        shared_down,
    )


def solution(mesh):
    in_specs = (
        P(("ep", "tp"), None),
        P(),
        P(("ep", "tp"), None),
        P(("ep", "tp"), None),
        P("ep", "tp", None),
        P("ep", "tp", None),
        P("ep", "tp", None),
        P("tp", None),
        P("tp", None),
        P("tp", None),
    )
    out_specs = P(("ep", "tp"), None)
    return jax.shard_map(body, mesh=mesh, in_specs=in_specs, out_specs=out_specs, check_vma=False)
```

time: 262 us -> 181 us (0.69)
  the two profiles are of different devices: /device:TPU:44 before, /device:TPU:5 now
where the time goes in v1:
time: 181 us; the launch traced here: 180 us
  Pallas kernels  172 us (95%)
  local copies, waits for them, and re-layouts  7.96 us (4%)
    pallas_call x1, Pallas kernels, body(): pl.pallas_call(kernel, out_shape=jax.ShapeDtypeStruct((TOK, D), BF), in_s...  172 us
    unnamed x21, local copies, waits for them, and re-layouts  7.96 us

profile of v1, /device:TPU:5, one launch (start us, length us, event | category | flops | bytes accessed | tf_op | source)
XLA Modules:
  0.0 180.3 jit_solution(4169432900472505859)
XLA Ops:
  0.0 0.0 copy-start.7
  0.0 0.0 copy-start.9
  0.0 0.0 copy-start.8
  0.0 0.7 copy-done.7
  0.7 0.0 copy-done.9
  0.7 0.0 copy-done.8
  0.7 0.0 copy-start
  0.7 1.0 copy-done
  1.8 0.0 copy-start.1
  1.8 0.9 copy-done.1
  2.7 0.0 copy-start.2
  2.7 0.9 copy-done.2
  3.6 0.0 copy-start.3
  3.6 0.9 copy-done.3
  4.5 0.0 copy-start.4
  4.5 0.9 copy-done.4
  5.4 0.0 copy-start.5
  5.4 0.9 copy-done.5
  6.3 0.0 copy-start.6
  6.3 0.9 copy-done.6
  7.2 172.3 %shard_map.100 = bf16[128,2048]{1,0:T(8,128)(2,1)S(1)} custom-call(bf16[128,2048]{1,0:T(8,128)(2,1)S(1)} %copy-done, f32[1,2048]{1,0:T(1,128)S(1)} %bitcast.9, s32[2,128]{1,0:T(2,128)S(1)} %bitcast.10, f32[2,128]{1,0:T(2,128)S(1)} %bitcast.11, bf16[2,16,2048]{2,1,0:T(8,128)(2,1)S(1)} %bitcast.6, bf16[2,16,2048]{2,1,0:T(8,128)(2,1)S(1)} %bitcast.7, ...), custom_call_target="tpu_custom_call" | custom-call | tf_op jit(solution)/shard_map/pallas_call | solution.py:297
  179.5 0.8 copy.12
Async XLA Ops:
  0.0 0.7 copy-start.7
  0.0 0.7 copy-start.9
  0.0 0.7 copy-start.8
  0.7 1.0 copy-start
  1.8 0.9 copy-start.1
  2.7 0.9 copy-start.2
  3.6 0.9 copy-start.3
  4.5 0.9 copy-start.4
  5.4 0.9 copy-start.5
  6.3 0.9 copy-start.6
